TPU v7x, 32 devices: a whole 2x2x4 slice. The times are simulated.
32 devices in a mesh: rep: 2 (over x), fs: 8 (over z, y), tp: 2 (over core).
Axes of the slice: x: 2, y: 2, z: 4, core: 2. Of those that a mesh axis runs over, the one named last changes fastest.
Arguments:
- hidden_in: bfloat16 [10240, 2048], P(('rep', 'fs'), 'tp'), may hold values from -6 to 6
- mix_gain: float32 [2048], replicated, may hold values from 0.1 to 1.9
- w_value: bfloat16 [2048, 1024], P('fs', 'tp'), may hold values from -0.125 to 0.125
- w_gate: bfloat16 [2048, 1024], P('fs', 'tp'), may hold values from -0.125 to 0.125
- conv_taps: float32 [31, 1024], P(None, 'tp'), may hold values from -5 to 5
- conv_bias: float32 [1024], P('tp'), may hold values from -3 to 3
- chan_gain: float32 [1024], P('tp'), may hold values from 0.1 to 1.9
- chan_bias: float32 [1024], P('tp'), may hold values from -3 to 3
- w_back: bfloat16 [1024, 2048], P('tp', 'fs'), may hold values from -0.1875 to 0.1875
- feed_gain: float32 [2048], replicated, may hold values from 0.1 to 1.9
- w_up: bfloat16 [2048, 8192], P(None, ('fs', 'tp')), may hold values from -0.125 to 0.125
- w_down: bfloat16 [8192, 2048], P(('fs', 'tp')), may hold values from -0.0625 to 0.0625
Outputs:
- layer_out: bfloat16 [10240, 2048], P(('rep', 'fs'), 'tp')
All inputs are finite; a program needn't handle non-finite values.
Results may differ from a plain program's by a relative error of at most 0.015.
Values may be sent and summed in bfloat16 or wider, within the bound.
A program may use at most 128 MiB of HBM per device.

v0:
```python
import jax
import jax.numpy as jnp
from jax import lax
from jax.sharding import Mesh, PartitionSpec as P

from jax.experimental import pallas as pl
from jax.experimental.pallas import tpu as pltpu


KW = 31
LEN = 128


SWAP = [(0, 1), (1, 0)]


def swap(value, axis):
    return lax.ppermute(value, axis, SWAP)


def ordered(own, other, index, axis):
    first = jnp.where(index == 0, own, other)
    return jnp.concatenate([first, jnp.where(index == 0, other, own)], axis=axis)


def own_first(array, index, axis):
    half = array.shape[axis] // 2
    return jnp.concatenate(
        [
            lax.dynamic_slice_in_dim(array, index * half, half, axis),
            lax.dynamic_slice_in_dim(array, (1 - index) * half, half, axis),
        ],
        axis=axis,
    )


def rms_norm(stream, gain):
    values = stream.astype(jnp.float32)
    scaled = values * lax.rsqrt(jnp.mean(values * values, axis=-1, keepdims=True) + 1e-06)
    return (scaled * gain).astype(jnp.bfloat16)


def causal_filter(gated, conv_taps, conv_bias):
    channels = gated.shape[1]
    blocks = gated.reshape(gated.shape[0] // LEN, LEN, channels)
    padded = jnp.pad(blocks, ((0, 0), (KW - 1, 0), (0, 0)))
    result = jnp.zeros_like(blocks) + conv_bias
    for tap_index in range(KW):
        result = result + conv_taps[tap_index] * padded[:, tap_index : tap_index + LEN]
    return result.reshape(gated.shape)


def plane_slots(piece):
    half = piece.shape[0] // 2
    from_rep = swap(piece, "rep")
    from_fy = swap(piece, "fy")
    diag_low = swap(from_rep[:half], "fy")
    diag_high = swap(from_fy[half:], "rep")
    return [piece, from_rep, from_fy, jnp.concatenate([diag_low, diag_high], axis=0)]


def full_features(slot):
    return jnp.concatenate([slot, swap(slot, "tp")], axis=1)


def tp_reduced(left, right):
    width = right.shape[1] // 2
    sent = jnp.dot(left, right[:, width:], preferred_element_type=jnp.float32)
    kept = jnp.dot(left, right[:, :width], preferred_element_type=jnp.float32)
    return kept + swap(sent.astype(jnp.bfloat16), "tp").astype(jnp.float32)


def plane_reduced(compute):
    diag = compute(3)
    half = diag.shape[0] // 2
    via_rep = swap(diag[:half].astype(jnp.bfloat16), "rep").astype(jnp.float32)
    via_fy = swap(diag[half:].astype(jnp.bfloat16), "fy").astype(jnp.float32)
    for_rep = compute(1)
    for_rep = jnp.concatenate([for_rep[:half], for_rep[half:] + via_fy], axis=0)
    from_rep = swap(for_rep.astype(jnp.bfloat16), "rep")
    for_fy = compute(2)
    for_fy = jnp.concatenate([for_fy[:half] + via_rep, for_fy[half:]], axis=0)
    from_fy = swap(for_fy.astype(jnp.bfloat16), "fy")
    return compute(0) + from_rep.astype(jnp.float32) + from_fy.astype(jnp.float32)


def block(
    hidden_in,
    mix_gain,
    w_value,
    w_gate,
    conv_taps,
    conv_bias,
    chan_gain,
    chan_bias,
    w_back,
    feed_gain,
    w_up,
    w_down,
):
    rep, fy, tp = lax.axis_index("rep"), lax.axis_index("fy"), lax.axis_index("tp")
    n_fz = lax.axis_size("fz")
    n_rep, n_fy, n_tp = lax.axis_size("rep"), lax.axis_size("fy"), lax.axis_size("tp")
    parts = n_rep * n_fy
    mine, theirs = rep * n_fy + fy, rep * n_fy + 1 - fy
    rows, back_cols = w_value.shape[0], w_back.shape[1]
    own_ch = w_value.shape[1] // parts

    def columns(array, which):
        return lax.dynamic_slice_in_dim(array, which * own_ch, own_ch, array.ndim - 1)

    def front_pack(which):
        packed_out = lax.dynamic_slice_in_dim(w_back, which * own_ch, own_ch, 0)
        pieces = [packed_out]
        if back_cols > own_ch:
            pieces = [
                packed_out[:, at : at + own_ch] for at in range(0, back_cols, own_ch)
            ]
        elif back_cols < own_ch:
            pieces = [packed_out.reshape(-1, own_ch)]
        return jnp.concatenate([columns(w_value, which), columns(w_gate, which)] + pieces, axis=0)

    received = swap(front_pack(theirs), "fy")
    slots = plane_slots(hidden_in)
    pair = ordered(front_pack(mine)[None], received[None], fy, 0)
    front = lax.all_gather(pair, "fz", axis=0, tiled=True)
    blocks = n_fz * n_fy
    w_in = own_first(
        jnp.concatenate(
            [
                front[:, :rows].reshape(blocks * rows, own_ch),
                front[:, rows : 2 * rows].reshape(blocks * rows, own_ch),
            ],
            axis=1,
        ),
        tp,
        0,
    )
    if back_cols >= own_ch:
        whole_back = front[:, 2 * rows :].reshape(blocks * (back_cols // own_ch), own_ch, own_ch)
    else:
        whole_back = front[:, 2 * rows :].reshape(blocks, own_ch, back_cols)
    whole_back = own_first(
        whole_back.transpose(1, 0, 2).reshape(own_ch, blocks * back_cols), tp, 1
    )

    own_ff = w_up.shape[1] // n_rep
    up_part = own_first(lax.dynamic_slice_in_dim(w_up, rep * own_ff, own_ff, 1), tp, 0)
    down_part = own_first(lax.dynamic_slice_in_dim(w_down, rep * own_ff, own_ff, 0), tp, 1)
    up = lax.all_gather(up_part, "fz", axis=1, tiled=True)
    down = lax.all_gather(down_part, "fz", axis=0, tiled=True)

    taps, bias = columns(conv_taps, mine), columns(conv_bias, mine)
    gain, shift = columns(chan_gain, mine), columns(chan_bias, mine)

    tokens = hidden_in.shape[0]
    mix_rolled, feed_rolled = own_first(mix_gain, tp, 0), own_first(feed_gain, tp, 0)
    gated = []
    for slot in slots:
        normed = rms_norm(full_features(slot), mix_rolled)
        both = jnp.dot(normed, w_in, preferred_element_type=jnp.float32)
        gated.append(both[:, :own_ch] * jax.nn.sigmoid(both[:, own_ch:]))
    filtered = causal_filter(jnp.concatenate(gated, axis=0), taps, bias)
    stats = jnp.stack([jnp.sum(filtered, axis=1), jnp.sum(filtered * filtered, axis=1)])
    stats = stats.reshape(2, 4, tokens)
    stats = stats + swap(stats, "tp")
    other = swap(stats, "rep")
    stats = stats + jnp.stack([other[:, at] for at in (1, 0, 3, 2)], axis=1)
    other = swap(stats, "fy")
    stats = stats + jnp.stack([other[:, at] for at in (2, 3, 0, 1)], axis=1)
    stats = stats.reshape(2, 4 * tokens) / (own_ch * parts * n_tp)
    chan_mean = stats[0][:, None]
    chan_var = stats[1][:, None] - chan_mean * chan_mean
    centred = (filtered - chan_mean) * lax.rsqrt(chan_var + 1e-05) * gain + shift
    act = jax.nn.silu(centred).astype(jnp.bfloat16)

    def mixed_share(index):
        return tp_reduced(act[index * tokens : (index + 1) * tokens], whole_back)

    mixed = plane_reduced(mixed_share)
    second = (hidden_in.astype(jnp.float32) + mixed).astype(jnp.bfloat16)

    hidden = []
    for slot in plane_slots(second):
        normed = rms_norm(full_features(slot), feed_rolled)
        up_proj = jnp.dot(normed, up, preferred_element_type=jnp.float32)
        hidden.append(jnp.square(jax.nn.relu(up_proj)).astype(jnp.bfloat16))
    hidden = list(lax.optimization_barrier(tuple(hidden)))

    def feed_share(index):
        return tp_reduced(hidden[index], down)

    feed = plane_reduced(feed_share)
    return (second.astype(jnp.float32) + feed).astype(jnp.bfloat16)


MESH = pl.DeviceIdType.MESH
LINE = 4
STAGES = 4
SENDS = 160
RECEIVES = 100
LANES = 128
HALO = 32


def fused_kernel(
    hidden_hbm,
    mix_gain,
    value_hbm,
    gate_hbm,
    taps,
    bias,
    chan_gain,
    chan_bias,
    back_hbm,
    feed_gain,
    up_hbm,
    down_hbm,
    out,
    stream,
    feat,
    front,
    back,
    halo,
    filtered,
    act,
    stats,
    stats_in,
    mix_out,
    mix_in,
    kept,
    second,
    square,
    square_in,
    up,
    down,
    hidden,
    pair_out,
    pair_in,
    plane_out,
    diag_in,
    rep_in,
    fy_in,
    local_sem,
    send_sem,
    recv_sem,
):
    f32, bf16 = jnp.float32, jnp.bfloat16
    rep, z, fy, tp = (lax.axis_index(name) for name in ("rep", "fz", "fy", "tp"))
    zs = (z, z + 1 - 2 * lax.rem(z, 2), lax.rem(z + LINE // 2, LINE), LINE - 1 - z)
    middle = lax.rem(z, LINE - 1) != 0
    to_rep, to_fy, to_tp = {"rep": 1 - rep}, {"fy": 1 - fy}, {"tp": 1 - tp}
    tokens, half = second.shape
    rows, chans = value_hbm.shape
    cols = chans // 2
    back_cols = back_hbm.shape[1]
    own_ff = up_hbm.shape[1] // 2
    ff = up.shape[1]
    width = 2 * half
    sent, slots = [], {}
    own_lanes = pl.ds(pl.multiple_of(tp * half, half), half)

    barrier = pltpu.get_barrier_semaphore()
    partners = [to_rep, to_fy, to_tp] + [{"fz": zs[at]} for at in range(1, LINE)]
    for partner in partners:
        pl.semaphore_signal(barrier, inc=1, device_id=partner, device_id_type=MESH)
    pl.semaphore_wait(barrier, len(partners))

    def slot(key):
        if key not in slots:
            slots[key] = len(slots)
            assert len(slots) <= RECEIVES
        return recv_sem.at[slots[key]]

    def push(key, src, device, dst=None, when=None):
        place = send_sem.at[len(sent)]
        arrive = slot(key)

        def copy():
            return pltpu.make_async_remote_copy(
                src_ref=src,
                dst_ref=src if dst is None else dst,
                send_sem=place,
                recv_sem=arrive,
                device_id=device,
                device_id_type=MESH,
            )

        sent.append((copy, when))
        assert len(sent) <= SENDS
        if when is None:
            copy().start()
        else:
            pl.when(when)(lambda: copy().start())

    def recv(key, ref):
        pltpu.make_async_remote_copy(
            src_ref=ref,
            dst_ref=ref,
            send_sem=send_sem.at[0],
            recv_sem=slot(key),
            device_id=to_tp,
            device_id_type=MESH,
        ).wait_recv()

    def local(index, pairs):
        for src, dst in pairs:
            pltpu.make_async_copy(src, dst, local_sem.at[index]).start()

    def local_wait(index, ref):
        pltpu.make_async_copy(ref, ref, local_sem.at[index]).wait()

    def block(index, which, size):
        return pl.ds(pl.multiple_of((zs[index] * 2 + which) * size, size), size)

    def front_half(index, which, side):
        return front.at[side, :, block(index, which, rows), :]

    def front_block(index, which):
        return front.at[:, :, block(index, which, rows), :]

    back_side = pl.ds(pl.multiple_of(rep * (chans // 2), chans // 2), chans // 2)
    back_far = pl.ds(pl.multiple_of((1 - rep) * (chans // 2), chans // 2), chans // 2)

    def back_half(index, which, side):
        return back.at[side, block(index, which, back_cols)]

    def back_block(index, which):
        return back.at[:, block(index, which, back_cols)]

    def unit(index):
        return pl.ds(pl.multiple_of(zs[index] * own_ff, own_ff), own_ff)

    up_rows = width // 2

    def up_piece(part):
        return lambda index: up.at[part * up_rows : (part + 1) * up_rows, unit(index)]

    step = half // STAGES

    def down_piece(part):
        return lambda index: down.at[:, unit(index), part * step : (part + 1) * step]

    def line_send(key, piece):
        push((key, 2), piece(0), {"fz": zs[2]})
        push((key, 3), piece(0), {"fz": zs[3]}, when=middle)
        push((key, 1), piece(0), {"fz": zs[1]})

    def line_relay(key, piece):
        recv((key, 2), piece(2))
        push((key, 3), piece(2), {"fz": zs[1]}, when=middle)

    local(0, [(hidden_hbm, stream.at[:, own_lanes])])
    push("hid", hidden_hbm, to_tp, stream.at[:, own_lanes])
    mine = block(0, fy, rows)
    local(
        1,
        [
            (hbm.at[:, side * cols : (side + 1) * cols], front.at[side, kind, mine, :])
            for side in range(2)
            for kind, hbm in enumerate((value_hbm, gate_hbm))
        ],
    )
    local(2, [(back_hbm, back_block(0, fy))])
    ff_part = pl.ds(pl.multiple_of(rep * own_ff, own_ff), own_ff)
    local(3, [(up_hbm.at[:, ff_part], up.at[:, unit(0)])])
    local(
        4,
        [
            (down_hbm.at[ff_part, side * half : (side + 1) * half], down.at[side, unit(0), :])
            for side in range(2)
        ],
    )

    local_wait(1, front_block(0, fy))
    line_send("zf", lambda index: front_half(index, fy, rep))
    push(("yf", 0), front_block(0, fy), to_fy)
    local_wait(2, back_block(0, fy))
    line_send("zb", lambda index: back_half(index, fy, back_side))

    halo[:, :HALO, :] = jnp.zeros((halo.shape[0], HALO, halo.shape[2]), f32)
    local_wait(0, stream.at[:, own_lanes])
    recv("hid", stream.at[:, pl.ds(pl.multiple_of((1 - tp) * half, half), half)])

    def norm_rows(at, carry):
        place = pl.ds(pl.multiple_of(at * 32, 32), 32)
        values = stream[place, :].astype(f32)
        scale = lax.rsqrt(jnp.sum(values * values, axis=-1, keepdims=True) / width + 1e-06)
        feat[0, place, :] = (values * scale * mix_gain[...]).astype(bf16)
        return carry

    lax.fori_loop(0, tokens // 32, norm_rows, 0)

    def front_on(index):
        push(("yf", index), front_half(index, fy, rep), to_fy)
        push(("xf", 0, index), front_half(index, fy, rep), to_rep)

    def front_turn(index):
        recv(("yf", index), front_half(index, 1 - fy, rep))
        push(("xf", 1, index), front_half(index, 1 - fy, rep), to_rep)

    def back_on(index):
        push(("yb", index), back_half(index, fy, back_side), to_fy)
        push(("xb", 0, index), back_half(index, fy, back_side), to_rep)

    def back_turn(index):
        recv(("yb", index), back_half(index, 1 - fy, back_side))
        push(("xb", 1, index), back_half(index, 1 - fy, back_side), to_rep)

    recv(("zf", 1), front_half(1, fy, rep))
    front_on(1)
    line_relay("zf", lambda index: front_half(index, fy, rep))
    front_on(2)
    front_turn(1)
    recv(("zf", 3), front_half(3, fy, rep))
    front_on(3)
    front_turn(2)
    push(("yb", 0), back_block(0, fy), to_fy)
    recv(("zb", 1), back_half(1, fy, back_side))
    line_relay("zb", lambda index: back_half(index, fy, back_side))
    local_wait(3, up.at[:, unit(0)])
    line_send(("up", 0), up_piece(0))
    front_turn(3)
    back_on(1)
    back_on(2)
    recv(("zb", 3), back_half(3, fy, back_side))
    back_on(3)
    line_send(("up", 1), up_piece(1))

    recv(("yf", 0), front_block(0, 1 - fy))
    for index in range(1, LINE):
        recv(("xf", 0, index), front_half(index, fy, 1 - rep))
        recv(("xf", 1, index), front_half(index, 1 - fy, 1 - rep))

    sequences = tokens // LEN
    for side in range(2):
        value = jnp.dot(feat[0], front[side, 0], preferred_element_type=f32)
        gate = jnp.dot(feat[0], front[side, 1], preferred_element_type=f32)
        gated = value * jax.nn.sigmoid(gate)
        halo[:, HALO:, side * cols : (side + 1) * cols] = gated.reshape(sequences, LEN, cols)

    for index in range(1, LINE):
        back_turn(index)

    def filter_sequence(at, carry):
        place = pl.ds(pl.multiple_of(at * LEN, LEN), LEN)
        total = jnp.zeros((LEN, LANES), f32)
        squares = jnp.zeros((LEN, LANES), f32)
        for lane in range(chans // LANES):
            lanes = slice(lane * LANES, (lane + 1) * LANES)
            result = jnp.zeros((LEN, LANES), f32) + bias[:, lanes]
            for tap in range(KW):
                start = HALO - KW + 1 + tap
                result = result + taps[tap : tap + 1, lanes] * halo[at, start : start + LEN, lanes]
            filtered[place, lanes] = result
            total = total + result
            squares = squares + result * result
        stats[0, place, :] = total
        stats[1, place, :] = squares
        return carry

    lax.fori_loop(0, sequences, filter_sequence, 0)
    push("stats", stats, to_tp, stats_in)
    line_relay(("up", 0), up_piece(0))
    recv("stats", stats_in)

    def act_rows(at, carry):
        place = pl.ds(pl.multiple_of(at * 32, 32), 32)
        count = 2 * chans
        mean = jnp.sum(stats[0, place, :] + stats_in[0, place, :], axis=-1, keepdims=True) / count
        second_moment = (
            jnp.sum(stats[1, place, :] + stats_in[1, place, :], axis=-1, keepdims=True) / count
        )
        scale = lax.rsqrt(second_moment - mean * mean + 1e-05)
        centred = (filtered[place, :] - mean) * scale * chan_gain[...] + chan_bias[...]
        act[place, :] = (centred * jax.nn.sigmoid(centred)).astype(bf16)
        return carry

    lax.fori_loop(0, tokens // 32, act_rows, 0)

    recv(("yb", 0), back_block(0, 1 - fy))
    for index in range(1, LINE):
        recv(("xb", 0, index), back_half(index, fy, back_far))
        recv(("xb", 1, index), back_half(index, 1 - fy, back_far))

    def back_lanes(side, part):
        return pl.ds(pl.multiple_of(side * half + part * step, step), step)

    for part in range(STAGES):
        lanes = slice(part * step, (part + 1) * step)
        product = jnp.dot(act[...], back[:, back_lanes(1 - tp, part)], preferred_element_type=f32)
        mix_out[:, lanes] = product.astype(bf16)
    push("mix", mix_out, to_tp, mix_in)
    for part in range(STAGES):
        kept[part] = jnp.dot(act[...], back[:, back_lanes(tp, part)], preferred_element_type=f32)
    recv("mix", mix_in)

    def second_rows(at, carry):
        place = pl.ds(pl.multiple_of(at * 32, 32), 32)
        squares = jnp.zeros((32, LANES), f32)
        for part in range(STAGES):
            lanes = slice(part * step, (part + 1) * step)
            source = pl.ds(pl.multiple_of(tp * half + part * step, step), step)
            mixed = kept[part, place, :] + mix_in[place, lanes].astype(f32)
            value = (stream[place, source].astype(f32) + mixed).astype(bf16)
            second[place, lanes] = value
            value = value.astype(f32)
            value = value * value
            for lane in range(step // LANES):
                squares = squares + value[:, lane * LANES : (lane + 1) * LANES]
        square[place, :] = squares
        return carry

    lax.fori_loop(0, tokens // 32, second_rows, 0)
    push("square", square, to_tp, square_in)
    local_wait(4, down.at[:, unit(0), :])
    line_send(("down", 0), down_piece(0))
    recv("square", square_in)

    def feed_rows(at, carry):
        place = pl.ds(pl.multiple_of(at * 32, 32), 32)
        mean = jnp.sum(square[place, :] + square_in[place, :], axis=-1, keepdims=True) / width
        scale = lax.rsqrt(mean + 1e-06)
        values = second[place, :].astype(f32) * scale * feed_gain[:, own_lanes]
        feat[0, place, own_lanes] = values.astype(bf16)
        return carry

    part_rows = tokens // 2

    def feat_part(index, part, lanes):
        return feat.at[index, part * part_rows : (part + 1) * part_rows, lanes]

    other_lanes = pl.ds(pl.multiple_of((1 - tp) * half, half), half)

    def share(index, part):
        push(("pair", index, part), feat_part(index, part, own_lanes), to_tp)

    def shared(index):
        for part in range(2):
            recv(("pair", index, part), feat_part(index, part, other_lanes))

    for part in range(2):
        lax.fori_loop(part * part_rows // 32, (part + 1) * part_rows // 32, feed_rows, 0)
        push(("rep", part), feat_part(0, part, own_lanes), to_rep, feat_part(1, part, own_lanes))
        push(("fy", part), feat_part(0, part, own_lanes), to_fy, feat_part(2, part, own_lanes))
        share(0, part)

    def up_slot(index):
        shared(index)
        for part in range(ff // step):
            lanes = slice(part * step, (part + 1) * step)
            product = jnp.dot(feat[index], up[:, lanes], preferred_element_type=f32)
            hidden[index, :, lanes] = jnp.square(jnp.maximum(product, 0.0)).astype(bf16)

    recv(("rep", 0), feat_part(1, 0, own_lanes))
    push(("diag", 0), feat_part(1, 0, own_lanes), to_fy, feat_part(3, 0, own_lanes))
    share(1, 0)
    recv(("fy", 0), feat_part(2, 0, own_lanes))
    share(2, 0)
    line_relay(("up", 1), up_piece(1))
    line_send(("down", 1), down_piece(1))
    recv(("rep", 1), feat_part(1, 1, own_lanes))
    share(1, 1)
    recv(("fy", 1), feat_part(2, 1, own_lanes))
    push(("diag", 1), feat_part(2, 1, own_lanes), to_rep, feat_part(3, 1, own_lanes))
    share(2, 1)
    for part in range(2):
        for index in (1, 3):
            recv((("up", part), index), up_piece(part)(index))
    up_slot(0)
    up_slot(1)
    recv(("diag", 0), feat_part(3, 0, own_lanes))
    share(3, 0)
    line_relay(("down", 0), down_piece(0))
    up_slot(2)
    recv(("diag", 1), feat_part(3, 1, own_lanes))
    share(3, 1)
    up_slot(3)

    def products(stage, index):
        lanes = slice(stage * step, (stage + 1) * step)
        product = jnp.dot(hidden[index], down[1 - tp, :, lanes], preferred_element_type=f32)
        pair_out[index, :, lanes] = product.astype(bf16)
        push(
            ("sum", index, stage),
            pair_out.at[index, :, lanes],
            to_tp,
            pair_in.at[index, :, lanes],
        )
        kept[index] = jnp.dot(hidden[index], down[tp, :, lanes], preferred_element_type=f32)

    def paired(stage, index, first, last):
        lanes = slice(stage * step, (stage + 1) * step)
        return kept[index, first:last, :] + pair_in[index, first:last, lanes].astype(f32)

    for stage in range(STAGES):
        lanes = slice(stage * step, (stage + 1) * step)
        piece = down_piece(stage)
        if stage + 2 < STAGES:
            line_send(("down", stage + 2), down_piece(stage + 2))
        for index in (1, 3):
            recv((("down", stage), index), piece(index))
        whole = slice(stage * step, (stage + 1) * step)
        products(stage, 3)
        products(stage, 1)
        recv(("sum", 3, stage), pair_in.at[3, :, whole])
        plane_out[2, :, lanes] = paired(stage, 3, 0, tokens).astype(bf16)
        push(
            ("far", 0, stage),
            plane_out.at[2, :part_rows, whole],
            to_rep,
            diag_in.at[0, :, whole],
        )
        push(
            ("far", 1, stage),
            plane_out.at[2, part_rows:, whole],
            to_fy,
            diag_in.at[1, :, whole],
        )
        products(stage, 2)
        products(stage, 0)
        recv(("sum", 1, stage), pair_in.at[1, :, whole])
        plane_out[0, :part_rows, lanes] = paired(stage, 1, 0, part_rows).astype(bf16)
        recv(("far", 1, stage), diag_in.at[1, :, whole])
        plane_out[0, part_rows:, lanes] = (
            paired(stage, 1, part_rows, tokens) + diag_in[1, :, lanes].astype(f32)
        ).astype(bf16)
        push(("near", 0, stage), plane_out.at[0, :, whole], to_rep, rep_in.at[:, whole])
        recv(("sum", 2, stage), pair_in.at[2, :, whole])
        plane_out[1, part_rows:, lanes] = paired(stage, 2, part_rows, tokens).astype(bf16)
        recv(("far", 0, stage), diag_in.at[0, :, whole])
        plane_out[1, :part_rows, lanes] = (
            paired(stage, 2, 0, part_rows) + diag_in[0, :, lanes].astype(f32)
        ).astype(bf16)
        push(("near", 1, stage), plane_out.at[1, :, whole], to_fy, fy_in.at[:, whole])
        recv(("sum", 0, stage), pair_in.at[0, :, whole])
        if stage + 1 < STAGES:
            line_relay(("down", stage + 1), down_piece(stage + 1))
        recv(("near", 0, stage), rep_in.at[:, whole])
        recv(("near", 1, stage), fy_in.at[:, whole])
        feed = paired(stage, 0, 0, tokens)
        feed = feed + rep_in[:, lanes].astype(f32) + fy_in[:, lanes].astype(f32)
        out[:, lanes] = (second[:, lanes].astype(f32) + feed).astype(bf16)

    for copy, when in sent:
        if when is None:
            copy().wait_send()
        else:
            pl.when(when)(lambda copy=copy: copy().wait_send())


def fused(*arrays):
    hidden_in, mix_gain, w_value, w_gate, taps, bias, gain, shift, w_back, feed_gain, w_up, w_down = arrays
    tokens, half = hidden_in.shape
    _, chans = w_value.shape
    width, ff = 2 * half, w_up.shape[1] // 2 * LINE
    bf16, f32 = jnp.bfloat16, jnp.float32
    vmem, hbm = pl.BlockSpec(memory_space=pltpu.VMEM), pl.BlockSpec(memory_space=pltpu.HBM)
    step = half // STAGES
    scratch = [
        ((tokens, width), bf16),
        ((4, tokens, width), bf16),
        ((2, 2, width, chans // 2), bf16),
        ((chans, width), bf16),
        ((tokens // LEN, HALO + LEN, chans), f32),
        ((tokens, chans), f32),
        ((tokens, chans), bf16),
        ((2, tokens, LANES), f32),
        ((2, tokens, LANES), f32),
        ((tokens, half), bf16),
        ((tokens, half), bf16),
        ((STAGES, tokens, step), f32),
        ((tokens, half), bf16),
        ((tokens, LANES), f32),
        ((tokens, LANES), f32),
        ((width, ff), bf16),
        ((2, ff, half), bf16),
        ((4, tokens, ff), bf16),
        ((4, tokens, half), bf16),
        ((4, tokens, half), bf16),
        ((3, tokens, half), bf16),
        ((2, tokens // 2, half), bf16),
        ((tokens, half), bf16),
        ((tokens, half), bf16),
    ]
    return pl.pallas_call(
        fused_kernel,
        out_shape=jax.ShapeDtypeStruct((tokens, half), bf16),
        in_specs=[hbm, vmem, hbm, hbm, vmem, vmem, vmem, vmem, hbm, vmem, hbm, hbm],
        out_specs=vmem,
        scratch_shapes=[pltpu.VMEM(shape, kind) for shape, kind in scratch]
        + [
            pltpu.SemaphoreType.DMA((5,)),
            pltpu.SemaphoreType.DMA((SENDS,)),
            pltpu.SemaphoreType.DMA((RECEIVES,)),
        ],
        compiler_params=pltpu.CompilerParams(
            collective_id=0, has_side_effects=True, vmem_limit_bytes=67043328
        ),
    )(
        hidden_in,
        mix_gain[None],
        w_value,
        w_gate,
        taps,
        bias[None],
        gain[None],
        shift[None],
        w_back,
        feed_gain[None],
        w_up,
        w_down,
    )


def fits(mesh):
    return mesh.shape["rep"] == 2 and mesh.shape["fs"] == 2 * LINE and mesh.shape["tp"] == 2


def solution(mesh):
    n_rep, n_fs, n_tp = mesh.shape["rep"], mesh.shape["fs"], mesh.shape["tp"]
    split = Mesh(mesh.devices.reshape(n_rep, n_fs // 2, 2, n_tp), ("rep", "fz", "fy", "tp"))
    fs = ("fz", "fy")
    rows = P(("rep", "fz", "fy"), "tp")
    placed = (
        rows,
        P(),
        P(fs, "tp"),
        P(fs, "tp"),
        P(None, "tp"),
        P("tp"),
        P("tp"),
        P("tp"),
        P("tp", fs),
        P(),
        P(None, ("fz", "fy", "tp")),
        P(("fz", "fy", "tp"), None),
    )
    if fits(mesh):
        return jax.shard_map(fused, mesh=split, in_specs=placed, out_specs=rows, check_vma=False)
    return jax.shard_map(block, mesh=split, in_specs=placed, out_specs=rows, check_vma=False)
```

profile of v0, /device:TPU:0, one launch (start us, length us, event | category | flops | bytes accessed | tf_op | source)
XLA Modules:
  0.0 207.6 jit_solution(10959505546452690170)
XLA Ops:
  0.0 205.1 %shard_map.118 = bf16[640,1024]{1,0:T(8,128)(2,1)} custom-call(bf16[640,1024]{1,0:T(8,128)(2,1)} %hidden_hbm.1, f32[1,2048]{1,0:T(1,128)} %bitcast.5, bf16[256,512]{1,0:T(8,128)(2,1)} %value_hbm.1, bf16[256,512]{1,0:T(8,128)(2,1)} %gate_hbm.1, f32[31,512]{1,0:T(8,128)} %taps.1, f32[1,512]{1,0:T(1,128)} %bitcast.7, f32[1,512]{1,0:T(1,128)} %bitcast.8, ...), custom_call_target="tpu_custom_call" | custom-call | tf_op jit(solution)/shard_map/pallas_call | solution.py:686
  205.1 2.5 %copy.14 = bf16[640,1024]{1,0:T(8,128)(2,1)} copy(bf16[640,1024]{1,0:T(8,128)(2,1)} %shard_map.118) | data formatting | bytes 2621440
where the time goes:
time: 208 us
  Pallas kernels  205 us (99%)
  local copies, waits for them, and re-layouts  2.47 us (1%)
    pallas_call x1, Pallas kernels, fused(): pl.pallas_call(fused_kernel, out_shape=jax.ShapeDtypeStruct((tokens, half...  205 us

commit v1 on v0

--- a/solution.py
+++ b/solution.py
@@ -197,8 +197,8 @@
 MESH = pl.DeviceIdType.MESH
 LINE = 4
 STAGES = 4
-SENDS = 160
-RECEIVES = 100
+SENDS = 200
+RECEIVES = 140
 LANES = 128
 HALO = 32
 
@@ -244,24 +244,28 @@
     local_sem,
     send_sem,
     recv_sem,
+    pair_sem,
 ):
     f32, bf16 = jnp.float32, jnp.bfloat16
     rep, z, fy, tp = (lax.axis_index(name) for name in ("rep", "fz", "fy", "tp"))
-    zs = (z, z + 1 - 2 * lax.rem(z, 2), lax.rem(z + LINE // 2, LINE), LINE - 1 - z)
+    low = z // (LINE // 2)
+    near, far, across = z + 1 - 2 * lax.rem(z, 2), lax.rem(z + LINE // 2, LINE), LINE - 1 - z
+    zs = (z, near, LINE // 2 - low, (LINE - 1) * (1 - low))
     middle = lax.rem(z, LINE - 1) != 0
+    ends = lax.rem(z, LINE - 1) == 0
     to_rep, to_fy, to_tp = {"rep": 1 - rep}, {"fy": 1 - fy}, {"tp": 1 - tp}
+    to_line = {"fz": near}
     tokens, half = second.shape
     rows, chans = value_hbm.shape
     cols = chans // 2
     back_cols = back_hbm.shape[1]
     own_ff = up_hbm.shape[1] // 2
-    ff = up.shape[1]
     width = 2 * half
-    sent, slots = [], {}
+    sent, slots, result = [], {}, mix_in
     own_lanes = pl.ds(pl.multiple_of(tp * half, half), half)
 
     barrier = pltpu.get_barrier_semaphore()
-    partners = [to_rep, to_fy, to_tp] + [{"fz": zs[at]} for at in range(1, LINE)]
+    partners = [to_rep, to_fy, to_tp] + [{"fz": at} for at in (near, far, across)]
     for partner in partners:
         pl.semaphore_signal(barrier, inc=1, device_id=partner, device_id_type=MESH)
     pl.semaphore_wait(barrier, len(partners))
@@ -293,15 +297,23 @@
         else:
             pl.when(when)(lambda: copy().start())
 
-    def recv(key, ref):
-        pltpu.make_async_remote_copy(
-            src_ref=ref,
-            dst_ref=ref,
-            send_sem=send_sem.at[0],
-            recv_sem=slot(key),
-            device_id=to_tp,
-            device_id_type=MESH,
-        ).wait_recv()
+    def recv(key, ref, when=None):
+        arrive = slot(key)
+
+        def wait():
+            pltpu.make_async_remote_copy(
+                src_ref=ref,
+                dst_ref=ref,
+                send_sem=send_sem.at[0],
+                recv_sem=arrive,
+                device_id=to_tp,
+                device_id_type=MESH,
+            ).wait_recv()
+
+        if when is None:
+            wait()
+        else:
+            pl.when(when)(wait)
 
     def local(index, pairs):
         for src, dst in pairs:
@@ -328,27 +340,49 @@
     def back_block(index, which):
         return back.at[:, block(index, which, back_cols)]
 
-    def unit(index):
-        return pl.ds(pl.multiple_of(zs[index] * own_ff, own_ff), own_ff)
-
+    step = half // STAGES
     up_rows = width // 2
-
-    def up_piece(part):
-        return lambda index: up.at[part * up_rows : (part + 1) * up_rows, unit(index)]
-
-    step = half // STAGES
-
-    def down_piece(part):
-        return lambda index: down.at[:, unit(index), part * step : (part + 1) * step]
+    given = pl.ds(pl.multiple_of(rep * own_ff, own_ff), own_ff)
+    taken = pl.ds(pl.multiple_of(2 * own_ff + rep * own_ff, own_ff), own_ff)
+    turned = pl.ds(pl.multiple_of(3 * own_ff - rep * own_ff, own_ff), own_ff)
+
+    def up_piece(part, units):
+        return up.at[part * up_rows : (part + 1) * up_rows, units]
+
+    def down_piece(part, units):
+        return down.at[:, units, cuts[part] : cuts[part + 1]]
+
+    cuts = [at * step for at in range(STAGES)] + [half - step // 2, half]
+    stages = len(cuts) - 1
+    early = 4
+    flow = [("up", part, up_piece) for part in range(2)]
+    flow += [("down", part, down_piece) for part in range(stages)]
+
+    def cross_send(at, when=None):
+        name, part, piece = flow[at]
+        push((name, part, "z"), piece(part, given), {"fz": across}, piece(part, taken), when=when)
+
+    def cross_turn(at, when):
+        name, part, piece = flow[at]
+        recv((name, part, "z"), piece(part, taken), when=when)
+        push((name, part, "x"), piece(part, taken), to_rep, when=when)
+
+    def cross_last(at):
+        name, part, piece = flow[at]
+        recv((name, part, "x"), piece(part, turned))
 
     def line_send(key, piece):
-        push((key, 2), piece(0), {"fz": zs[2]})
-        push((key, 3), piece(0), {"fz": zs[3]}, when=middle)
-        push((key, 1), piece(0), {"fz": zs[1]})
+        push((key, 2), piece(0), {"fz": far}, when=middle)
+        push((key, 3), piece(0), {"fz": far}, when=ends)
+        push((key, 2), piece(0), {"fz": across}, when=middle)
+        push((key, 1), piece(0), {"fz": near})
 
     def line_relay(key, piece):
-        recv((key, 2), piece(2))
-        push((key, 3), piece(2), {"fz": zs[1]}, when=middle)
+        recv((key, 3), piece(3), when=middle)
+        push((key, 3), piece(3), {"fz": near}, when=middle)
+
+    def line_last(key, piece):
+        recv((key, 3), piece(3), when=ends)
 
     local(0, [(hidden_hbm, stream.at[:, own_lanes])])
     push("hid", hidden_hbm, to_tp, stream.at[:, own_lanes])
@@ -362,19 +396,20 @@
         ],
     )
     local(2, [(back_hbm, back_block(0, fy))])
-    ff_part = pl.ds(pl.multiple_of(rep * own_ff, own_ff), own_ff)
-    local(3, [(up_hbm.at[:, ff_part], up.at[:, unit(0)])])
+    own_units = pl.ds(0, 2 * own_ff)
+    local(3, [(up_hbm, up.at[:, own_units])])
     local(
         4,
         [
-            (down_hbm.at[ff_part, side * half : (side + 1) * half], down.at[side, unit(0), :])
+            (down_hbm.at[:, side * half : (side + 1) * half], down.at[side, own_units, :])
             for side in range(2)
         ],
     )
 
     local_wait(1, front_block(0, fy))
     line_send("zf", lambda index: front_half(index, fy, rep))
-    push(("yf", 0), front_block(0, fy), to_fy)
+    push(("yf", 0, 0), front_half(0, fy, 0), to_fy)
+    push(("yf", 0, 1), front_half(0, fy, 1), to_fy, when=middle)
     local_wait(2, back_block(0, fy))
     line_send("zb", lambda index: back_half(index, fy, back_side))
 
@@ -391,9 +426,9 @@
 
     lax.fori_loop(0, tokens // 32, norm_rows, 0)
 
-    def front_on(index):
-        push(("yf", index), front_half(index, fy, rep), to_fy)
-        push(("xf", 0, index), front_half(index, fy, rep), to_rep)
+    def front_on(index, when=None):
+        push(("yf", index), front_half(index, fy, rep), to_fy, when=when)
+        push(("xf", 0, index), front_half(index, fy, rep), to_rep, when=when)
 
     def front_turn(index):
         recv(("yf", index), front_half(index, 1 - fy, rep))
@@ -407,30 +442,49 @@
         recv(("yb", index), back_half(index, 1 - fy, back_side))
         push(("xb", 1, index), back_half(index, 1 - fy, back_side), to_rep)
 
+    def front_cross():
+        recv(("xf", 0, 1), front_half(1, fy, 1 - rep))
+        push(("yf", "x"), front_half(1, fy, 1 - rep), to_fy)
+
+    def back_cross():
+        recv(("xb", 0, 1), back_half(1, fy, back_far))
+        push(("yb", "x"), back_half(1, fy, back_far), to_fy)
+
     recv(("zf", 1), front_half(1, fy, rep))
     front_on(1)
     line_relay("zf", lambda index: front_half(index, fy, rep))
+    front_on(3, middle)
+    recv(("zf", 2), front_half(2, fy, rep))
     front_on(2)
-    front_turn(1)
-    recv(("zf", 3), front_half(3, fy, rep))
-    front_on(3)
+    front_cross()
+    local_wait(3, up.at[:, own_units])
+    local_wait(4, down.at[:, own_units, :])
+    line_last("zf", lambda index: front_half(index, fy, rep))
+    front_on(3, ends)
+    push(("yf", 0, 1), front_half(0, fy, 1), to_fy, when=ends)
+    line_relay("zb", lambda index: back_half(index, fy, back_side))
     front_turn(2)
+    front_turn(3)
+    recv(("zb", 1), back_half(1, fy, back_side))
+    back_on(1)
+    recv(("zb", 2), back_half(2, fy, back_side))
+    back_on(2)
+    line_last("zb", lambda index: back_half(index, fy, back_side))
+    back_on(3)
+    pl.semaphore_signal(pair_sem, inc=1, device_id=to_tp, device_id_type=MESH)
     push(("yb", 0), back_block(0, fy), to_fy)
-    recv(("zb", 1), back_half(1, fy, back_side))
-    line_relay("zb", lambda index: back_half(index, fy, back_side))
-    local_wait(3, up.at[:, unit(0)])
-    line_send(("up", 0), up_piece(0))
-    front_turn(3)
-    back_on(1)
-    back_on(2)
-    recv(("zb", 3), back_half(3, fy, back_side))
-    back_on(3)
-    line_send(("up", 1), up_piece(1))
-
-    recv(("yf", 0), front_block(0, 1 - fy))
-    for index in range(1, LINE):
-        recv(("xf", 0, index), front_half(index, fy, 1 - rep))
-        recv(("xf", 1, index), front_half(index, 1 - fy, 1 - rep))
+    pl.semaphore_wait(pair_sem, 1)
+    for at in range(len(flow)):
+        cross_send(at, None if at < early else middle)
+
+    recv(("yf", 1), front_half(1, 1 - fy, rep))
+    recv(("yf", 0, 0), front_half(0, 1 - fy, 0))
+    recv(("yf", 0, 1), front_half(0, 1 - fy, 1))
+    recv(("xf", 0, 2), front_half(2, fy, 1 - rep))
+    recv(("xf", 1, 2), front_half(2, 1 - fy, 1 - rep))
+    recv(("yf", "x"), front_half(1, 1 - fy, 1 - rep))
+    recv(("xf", 0, 3), front_half(3, fy, 1 - rep))
+    recv(("xf", 1, 3), front_half(3, 1 - fy, 1 - rep))
 
     sequences = tokens // LEN
     for side in range(2):
@@ -438,9 +492,6 @@
         gate = jnp.dot(feat[0], front[side, 1], preferred_element_type=f32)
         gated = value * jax.nn.sigmoid(gate)
         halo[:, HALO:, side * cols : (side + 1) * cols] = gated.reshape(sequences, LEN, cols)
-
-    for index in range(1, LINE):
-        back_turn(index)
 
     def filter_sequence(at, carry):
         place = pl.ds(pl.multiple_of(at * LEN, LEN), LEN)
@@ -459,9 +510,14 @@
         stats[1, place, :] = squares
         return carry
 
-    lax.fori_loop(0, sequences, filter_sequence, 0)
+    middle_sequence = sequences - sequences // 2
+    lax.fori_loop(0, middle_sequence, filter_sequence, 0)
+    recv(("yb", 1), back_half(1, 1 - fy, back_side))
+    back_cross()
+    back_turn(2)
+    lax.fori_loop(middle_sequence, sequences, filter_sequence, 0)
+    back_turn(3)
     push("stats", stats, to_tp, stats_in)
-    line_relay(("up", 0), up_piece(0))
     recv("stats", stats_in)
 
     def act_rows(at, carry):
@@ -479,7 +535,8 @@
     lax.fori_loop(0, tokens // 32, act_rows, 0)
 
     recv(("yb", 0), back_block(0, 1 - fy))
-    for index in range(1, LINE):
+    recv(("yb", "x"), back_half(1, 1 - fy, back_far))
+    for index in range(2, LINE):
         recv(("xb", 0, index), back_half(index, fy, back_far))
         recv(("xb", 1, index), back_half(index, 1 - fy, back_far))
 
@@ -513,8 +570,6 @@
 
     lax.fori_loop(0, tokens // 32, second_rows, 0)
     push("square", square, to_tp, square_in)
-    local_wait(4, down.at[:, unit(0), :])
-    line_send(("down", 0), down_piece(0))
     recv("square", square_in)
 
     def feed_rows(at, carry):
@@ -541,44 +596,64 @@
 
     for part in range(2):
         lax.fori_loop(part * part_rows // 32, (part + 1) * part_rows // 32, feed_rows, 0)
-        push(("rep", part), feat_part(0, part, own_lanes), to_rep, feat_part(1, part, own_lanes))
+        push(("line", part), feat_part(0, part, own_lanes), to_line, feat_part(1, part, own_lanes))
         push(("fy", part), feat_part(0, part, own_lanes), to_fy, feat_part(2, part, own_lanes))
         share(0, part)
 
-    def up_slot(index):
-        shared(index)
-        for part in range(ff // step):
-            lanes = slice(part * step, (part + 1) * step)
+    def up_slot(index, side):
+        for part in range(2):
+            lanes = slice((2 * side + part) * own_ff, (2 * side + part + 1) * own_ff)
             product = jnp.dot(feat[index], up[:, lanes], preferred_element_type=f32)
             hidden[index, :, lanes] = jnp.square(jnp.maximum(product, 0.0)).astype(bf16)
 
-    recv(("rep", 0), feat_part(1, 0, own_lanes))
+    for at in range(early - 1):
+        cross_turn(at, ends)
+    shared(0)
+    up_slot(0, 0)
+    cross_turn(0, middle)
+    recv(("line", 0), feat_part(1, 0, own_lanes))
     push(("diag", 0), feat_part(1, 0, own_lanes), to_fy, feat_part(3, 0, own_lanes))
     share(1, 0)
     recv(("fy", 0), feat_part(2, 0, own_lanes))
     share(2, 0)
-    line_relay(("up", 1), up_piece(1))
-    line_send(("down", 1), down_piece(1))
-    recv(("rep", 1), feat_part(1, 1, own_lanes))
+    cross_turn(1, middle)
+    cross_turn(early - 1, ends)
+    recv(("line", 1), feat_part(1, 1, own_lanes))
     share(1, 1)
     recv(("fy", 1), feat_part(2, 1, own_lanes))
-    push(("diag", 1), feat_part(2, 1, own_lanes), to_rep, feat_part(3, 1, own_lanes))
+    push(("diag", 1), feat_part(2, 1, own_lanes), to_line, feat_part(3, 1, own_lanes))
+    for at in range(early, len(flow)):
+        cross_send(at, ends)
     share(2, 1)
-    for part in range(2):
-        for index in (1, 3):
-            recv((("up", part), index), up_piece(part)(index))
-    up_slot(0)
-    up_slot(1)
+    shared(1)
+    up_slot(1, 0)
+    shared(2)
+    up_slot(2, 0)
+    cross_turn(2, middle)
+    cross_last(0)
+    cross_last(1)
+    up_slot(0, 1)
     recv(("diag", 0), feat_part(3, 0, own_lanes))
     share(3, 0)
-    line_relay(("down", 0), down_piece(0))
-    up_slot(2)
+    up_slot(1, 1)
+    cross_turn(3, middle)
+    up_slot(2, 1)
     recv(("diag", 1), feat_part(3, 1, own_lanes))
     share(3, 1)
-    up_slot(3)
+    shared(3)
+    up_slot(3, 0)
+    up_slot(3, 1)
+
+    turn_rows = tokens * 3 // 10
+
+    def home(stage, index):
+        return index if index or stage % 2 == 0 else STAGES
+
+    def span(stage):
+        return slice(cuts[stage], cuts[stage + 1])
 
     def products(stage, index):
-        lanes = slice(stage * step, (stage + 1) * step)
+        lanes = span(stage)
         product = jnp.dot(hidden[index], down[1 - tp, :, lanes], preferred_element_type=f32)
         pair_out[index, :, lanes] = product.astype(bf16)
         push(
@@ -587,60 +662,81 @@
             to_tp,
             pair_in.at[index, :, lanes],
         )
-        kept[index] = jnp.dot(hidden[index], down[tp, :, lanes], preferred_element_type=f32)
+        product = jnp.dot(hidden[index], down[tp, :, lanes], preferred_element_type=f32)
+        kept[home(stage, index), :, : cuts[stage + 1] - cuts[stage]] = product
 
     def paired(stage, index, first, last):
-        lanes = slice(stage * step, (stage + 1) * step)
-        return kept[index, first:last, :] + pair_in[index, first:last, lanes].astype(f32)
-
-    for stage in range(STAGES):
-        lanes = slice(stage * step, (stage + 1) * step)
-        piece = down_piece(stage)
-        if stage + 2 < STAGES:
-            line_send(("down", stage + 2), down_piece(stage + 2))
-        for index in (1, 3):
-            recv((("down", stage), index), piece(index))
-        whole = slice(stage * step, (stage + 1) * step)
-        products(stage, 3)
-        products(stage, 1)
-        recv(("sum", 3, stage), pair_in.at[3, :, whole])
+        lanes = span(stage)
+        own = kept[home(stage, index), first:last, : cuts[stage + 1] - cuts[stage]]
+        return own + pair_in[index, first:last, lanes].astype(f32)
+
+    def finish(stage):
+        lanes = span(stage)
+        recv(("sum", 0, stage), pair_in.at[0, :, lanes])
+        recv(("near", 0, stage), rep_in.at[:, lanes])
+        recv(("near", 1, stage), fy_in.at[:, lanes])
+        feed = paired(stage, 0, 0, tokens)
+        feed = feed + rep_in[:, lanes].astype(f32) + fy_in[:, lanes].astype(f32)
+        result[:, lanes] = (second[:, lanes].astype(f32) + feed).astype(bf16)
+        local(5 + stage, [(result.at[:, lanes], out.at[:, lanes])])
+
+    def send_far(stage):
+        lanes = span(stage)
+        recv(("sum", 3, stage), pair_in.at[3, :, lanes])
         plane_out[2, :, lanes] = paired(stage, 3, 0, tokens).astype(bf16)
-        push(
-            ("far", 0, stage),
-            plane_out.at[2, :part_rows, whole],
-            to_rep,
-            diag_in.at[0, :, whole],
-        )
-        push(
-            ("far", 1, stage),
-            plane_out.at[2, part_rows:, whole],
-            to_fy,
-            diag_in.at[1, :, whole],
-        )
+        for part, (rows_of, device) in enumerate(
+            ((slice(0, turn_rows), to_line), (slice(turn_rows, tokens), to_fy))
+        ):
+            push(
+                ("far", part, stage),
+                plane_out.at[2, rows_of, lanes],
+                device,
+                diag_in.at[rows_of, lanes],
+            )
+
+    def send_near(stage):
+        lanes = span(stage)
+        recv(("sum", 1, stage), pair_in.at[1, :, lanes])
+        plane_out[0, :turn_rows, lanes] = paired(stage, 1, 0, turn_rows).astype(bf16)
+        recv(("far", 1, stage), diag_in.at[turn_rows:, lanes])
+        plane_out[0, turn_rows:, lanes] = (
+            paired(stage, 1, turn_rows, tokens) + diag_in[turn_rows:, lanes].astype(f32)
+        ).astype(bf16)
+        push(("near", 0, stage), plane_out.at[0, :, lanes], to_line, rep_in.at[:, lanes])
+        recv(("sum", 2, stage), pair_in.at[2, :, lanes])
+        plane_out[1, turn_rows:, lanes] = paired(stage, 2, turn_rows, tokens).astype(bf16)
+        recv(("far", 0, stage), diag_in.at[:turn_rows, lanes])
+        plane_out[1, :turn_rows, lanes] = (
+            paired(stage, 2, 0, turn_rows) + diag_in[:turn_rows, lanes].astype(f32)
+        ).astype(bf16)
+        push(("near", 1, stage), plane_out.at[1, :, lanes], to_fy, fy_in.at[:, lanes])
+
+    cross_last(2)
+    products(0, 3)
+    products(0, 1)
+    send_far(0)
+    for stage in range(stages):
+        last = stage + 1 == stages
+        if not last:
+            if stage == 0:
+                cross_turn(early, None)
+            cross_last(stage + 3)
+            products(stage + 1, 3)
         products(stage, 2)
         products(stage, 0)
-        recv(("sum", 1, stage), pair_in.at[1, :, whole])
-        plane_out[0, :part_rows, lanes] = paired(stage, 1, 0, part_rows).astype(bf16)
-        recv(("far", 1, stage), diag_in.at[1, :, whole])
-        plane_out[0, part_rows:, lanes] = (
-            paired(stage, 1, part_rows, tokens) + diag_in[1, :, lanes].astype(f32)
-        ).astype(bf16)
-        push(("near", 0, stage), plane_out.at[0, :, whole], to_rep, rep_in.at[:, whole])
-        recv(("sum", 2, stage), pair_in.at[2, :, whole])
-        plane_out[1, part_rows:, lanes] = paired(stage, 2, part_rows, tokens).astype(bf16)
-        recv(("far", 0, stage), diag_in.at[0, :, whole])
-        plane_out[1, :part_rows, lanes] = (
-            paired(stage, 2, 0, part_rows) + diag_in[0, :, lanes].astype(f32)
-        ).astype(bf16)
-        push(("near", 1, stage), plane_out.at[1, :, whole], to_fy, fy_in.at[:, whole])
-        recv(("sum", 0, stage), pair_in.at[0, :, whole])
-        if stage + 1 < STAGES:
-            line_relay(("down", stage + 1), down_piece(stage + 1))
-        recv(("near", 0, stage), rep_in.at[:, whole])
-        recv(("near", 1, stage), fy_in.at[:, whole])
-        feed = paired(stage, 0, 0, tokens)
-        feed = feed + rep_in[:, lanes].astype(f32) + fy_in[:, lanes].astype(f32)
-        out[:, lanes] = (second[:, lanes].astype(f32) + feed).astype(bf16)
+        if not last:
+            send_far(stage + 1)
+        send_near(stage)
+        if early + stage + 1 < len(flow):
+            cross_turn(early + stage + 1, None)
+        if not last:
+            products(stage + 1, 1)
+        if stage:
+            finish(stage - 1)
+    finish(stages - 1)
+    for stage in range(stages):
+        lanes = span(stage)
+        pltpu.make_async_copy(result.at[:, lanes], out.at[:, lanes], local_sem.at[5 + stage]).wait()
 
     for copy, when in sent:
         if when is None:
@@ -669,7 +765,7 @@
         ((2, tokens, LANES), f32),
         ((tokens, half), bf16),
         ((tokens, half), bf16),
-        ((STAGES, tokens, step), f32),
+        ((STAGES + 1, tokens, step), f32),
         ((tokens, half), bf16),
         ((tokens, LANES), f32),
         ((tokens, LANES), f32),
@@ -679,7 +775,7 @@
         ((4, tokens, half), bf16),
         ((4, tokens, half), bf16),
         ((3, tokens, half), bf16),
-        ((2, tokens // 2, half), bf16),
+        ((tokens, half), bf16),
         ((tokens, half), bf16),
         ((tokens, half), bf16),
     ]
@@ -687,12 +783,13 @@
         fused_kernel,
         out_shape=jax.ShapeDtypeStruct((tokens, half), bf16),
         in_specs=[hbm, vmem, hbm, hbm, vmem, vmem, vmem, vmem, hbm, vmem, hbm, hbm],
-        out_specs=vmem,
+        out_specs=hbm,
         scratch_shapes=[pltpu.VMEM(shape, kind) for shape, kind in scratch]
         + [
-            pltpu.SemaphoreType.DMA((5,)),
+            pltpu.SemaphoreType.DMA((6 + STAGES,)),
             pltpu.SemaphoreType.DMA((SENDS,)),
             pltpu.SemaphoreType.DMA((RECEIVES,)),
+            pltpu.SemaphoreType.REGULAR,
         ],
         compiler_params=pltpu.CompilerParams(
             collective_id=0, has_side_effects=True, vmem_limit_bytes=67043328

time: 208 us -> 188 us (0.904)
  Pallas kernels: 205 us -> 184 us
    pallas_call x1, Pallas kernels: 205 us -> 184 us  [fused(): pl.pallas_call(fused_kernel, out_shape=jax.ShapeDtypeStruct((tokens, half...]
where the time goes in v1:
time: 188 us; the launch traced here: 187 us
  Pallas kernels  184 us (98%)
  local copies, waits for them, and re-layouts  2.47 us (1%)
    pallas_call x1, Pallas kernels, fused(): pl.pallas_call(fused_kernel, out_shape=jax.ShapeDtypeStruct((tokens, half...  184 us

profile of v1, /device:TPU:0, one launch (start us, length us, event | category | flops | bytes accessed | tf_op | source)
XLA Modules:
  0.0 187.0 jit_solution(12111569427619080257)
XLA Ops:
  0.0 184.5 %shard_map.118 = bf16[640,1024]{1,0:T(8,128)(2,1)} custom-call(bf16[640,1024]{1,0:T(8,128)(2,1)} %hidden_hbm.1, f32[1,2048]{1,0:T(1,128)} %bitcast.5, bf16[256,512]{1,0:T(8,128)(2,1)} %value_hbm.1, bf16[256,512]{1,0:T(8,128)(2,1)} %gate_hbm.1, f32[31,512]{1,0:T(8,128)} %taps.1, f32[1,512]{1,0:T(1,128)} %bitcast.7, f32[1,512]{1,0:T(1,128)} %bitcast.8, ...), custom_call_target="tpu_custom_call" | custom-call | tf_op jit(solution)/shard_map/pallas_call | solution.py:782
  184.5 2.5 %copy.14 = bf16[640,1024]{1,0:T(8,128)(2,1)} copy(bf16[640,1024]{1,0:T(8,128)(2,1)} %shard_map.118) | data formatting | bytes 2621440

commit v2 on v1

--- a/solution.py
+++ b/solution.py
@@ -201,6 +201,7 @@
 RECEIVES = 140
 LANES = 128
 HALO = 32
+SUBLANES = 8
 
 
 def fused_kernel(
@@ -444,7 +445,7 @@
 
     def front_cross():
         recv(("xf", 0, 1), front_half(1, fy, 1 - rep))
-        push(("yf", "x"), front_half(1, fy, 1 - rep), to_fy)
+        push(("yf", "x"), front.at[1 - rep, 0, block(1, fy, rows), :], to_fy)
 
     def back_cross():
         recv(("xb", 0, 1), back_half(1, fy, back_far))
@@ -456,11 +457,13 @@
     front_on(3, middle)
     recv(("zf", 2), front_half(2, fy, rep))
     front_on(2)
-    front_cross()
+    recv(("yf", 1), front_half(1, 1 - fy, rep))
+    push(("xf", "y"), front.at[rep, 1, block(1, 1 - fy, rows), :], to_rep)
     local_wait(3, up.at[:, own_units])
     local_wait(4, down.at[:, own_units, :])
     line_last("zf", lambda index: front_half(index, fy, rep))
     front_on(3, ends)
+    front_cross()
     push(("yf", 0, 1), front_half(0, fy, 1), to_fy, when=ends)
     line_relay("zb", lambda index: back_half(index, fy, back_side))
     front_turn(2)
@@ -477,12 +480,12 @@
     for at in range(len(flow)):
         cross_send(at, None if at < early else middle)
 
-    recv(("yf", 1), front_half(1, 1 - fy, rep))
     recv(("yf", 0, 0), front_half(0, 1 - fy, 0))
     recv(("yf", 0, 1), front_half(0, 1 - fy, 1))
     recv(("xf", 0, 2), front_half(2, fy, 1 - rep))
     recv(("xf", 1, 2), front_half(2, 1 - fy, 1 - rep))
-    recv(("yf", "x"), front_half(1, 1 - fy, 1 - rep))
+    recv(("yf", "x"), front.at[1 - rep, 0, block(1, 1 - fy, rows), :])
+    recv(("xf", "y"), front.at[1 - rep, 1, block(1, 1 - fy, rows), :])
     recv(("xf", 0, 3), front_half(3, fy, 1 - rep))
     recv(("xf", 1, 3), front_half(3, 1 - fy, 1 - rep))
 
@@ -500,9 +503,17 @@
         for lane in range(chans // LANES):
             lanes = slice(lane * LANES, (lane + 1) * LANES)
             result = jnp.zeros((LEN, LANES), f32) + bias[:, lanes]
-            for tap in range(KW):
-                start = HALO - KW + 1 + tap
-                result = result + taps[tap : tap + 1, lanes] * halo[at, start : start + LEN, lanes]
+            for shift in range(SUBLANES):
+                size = LEN + SUBLANES if shift else LEN
+                part = None
+                for start in range(0, HALO + 1, SUBLANES):
+                    tap = start + shift - (HALO - KW + 1)
+                    if 0 <= tap < KW:
+                        term = taps[tap : tap + 1, lanes] * halo[at, start : start + size, lanes]
+                        part = term if part is None else part + term
+                if shift:
+                    part = pltpu.roll(part, size - shift, 0)[:LEN]
+                result = result + part
             filtered[place, lanes] = result
             total = total + result
             squares = squares + result * result
@@ -582,17 +593,20 @@
 
     part_rows = tokens // 2
 
-    def feat_part(index, part, lanes):
-        return feat.at[index, part * part_rows : (part + 1) * part_rows, lanes]
+    bounds = {index: (0, part_rows, tokens) for index in range(3)}
+    bounds[3] = (0, part_rows, part_rows + part_rows // 2, tokens)
+
+    def feat_part(index, part, lanes, like=None):
+        edges = bounds[index if like is None else like]
+        return feat.at[index, edges[part] : edges[part + 1], lanes]
 
     other_lanes = pl.ds(pl.multiple_of((1 - tp) * half, half), half)
 
     def share(index, part):
         push(("pair", index, part), feat_part(index, part, own_lanes), to_tp)
 
-    def shared(index):
-        for part in range(2):
-            recv(("pair", index, part), feat_part(index, part, other_lanes))
+    def shared(index, part):
+        recv(("pair", index, part), feat_part(index, part, other_lanes))
 
     for part in range(2):
         lax.fori_loop(part * part_rows // 32, (part + 1) * part_rows // 32, feed_rows, 0)
@@ -600,15 +614,20 @@
         push(("fy", part), feat_part(0, part, own_lanes), to_fy, feat_part(2, part, own_lanes))
         share(0, part)
 
-    def up_slot(index, side):
-        for part in range(2):
-            lanes = slice((2 * side + part) * own_ff, (2 * side + part + 1) * own_ff)
-            product = jnp.dot(feat[index], up[:, lanes], preferred_element_type=f32)
-            hidden[index, :, lanes] = jnp.square(jnp.maximum(product, 0.0)).astype(bf16)
+    def up_slot(index, side, part=None):
+        first, last = (0, tokens) if part is None else bounds[index][part : part + 2]
+        for piece in range(2):
+            lanes = slice((2 * side + piece) * own_ff, (2 * side + piece + 1) * own_ff)
+            product = jnp.dot(
+                feat[index, first:last, :], up[:, lanes], preferred_element_type=f32
+            )
+            product = jnp.square(jnp.maximum(product, 0.0))
+            hidden[index, first:last, lanes] = product.astype(bf16)
 
     for at in range(early - 1):
         cross_turn(at, ends)
-    shared(0)
+    shared(0, 0)
+    shared(0, 1)
     up_slot(0, 0)
     cross_turn(0, middle)
     recv(("line", 0), feat_part(1, 0, own_lanes))
@@ -621,13 +640,21 @@
     recv(("line", 1), feat_part(1, 1, own_lanes))
     share(1, 1)
     recv(("fy", 1), feat_part(2, 1, own_lanes))
-    push(("diag", 1), feat_part(2, 1, own_lanes), to_line, feat_part(3, 1, own_lanes))
+    for part in (1, 2):
+        push(
+            ("diag", part),
+            feat_part(2, part, own_lanes, 3),
+            to_line,
+            feat_part(3, part, own_lanes),
+        )
     for at in range(early, len(flow)):
         cross_send(at, ends)
     share(2, 1)
-    shared(1)
+    shared(1, 0)
+    shared(1, 1)
     up_slot(1, 0)
-    shared(2)
+    shared(2, 0)
+    shared(2, 1)
     up_slot(2, 0)
     cross_turn(2, middle)
     cross_last(0)
@@ -638,11 +665,16 @@
     up_slot(1, 1)
     cross_turn(3, middle)
     up_slot(2, 1)
-    recv(("diag", 1), feat_part(3, 1, own_lanes))
-    share(3, 1)
-    shared(3)
-    up_slot(3, 0)
-    up_slot(3, 1)
+    shared(3, 0)
+    for side in range(2):
+        up_slot(3, side, 0)
+    for part in (1, 2):
+        recv(("diag", part), feat_part(3, part, own_lanes))
+        share(3, part)
+    for part in (1, 2):
+        shared(3, part)
+        for side in range(2):
+            up_slot(3, side, part)
 
     turn_rows = tokens * 3 // 10
 

time: 188 us -> 183 us (0.973)
  Pallas kernels: 184 us -> 180 us
    pallas_call x1, Pallas kernels: 184 us -> 180 us  [fused(): pl.pallas_call(fused_kernel, out_shape=jax.ShapeDtypeStruct((tokens, half...]
where the time goes in v2:
time: 183 us; the launch traced here: 182 us
  Pallas kernels  180 us (98%)
  local copies, waits for them, and re-layouts  2.47 us (1%)
    pallas_call x1, Pallas kernels, fused(): pl.pallas_call(fused_kernel, out_shape=jax.ShapeDtypeStruct((tokens, half...  180 us

profile of v2, /device:TPU:0, one launch (start us, length us, event | category | flops | bytes accessed | tf_op | source)
XLA Modules:
  0.0 182.4 jit_solution(11550498360806463703)
XLA Ops:
  0.0 179.9 %shard_map.118 = bf16[640,1024]{1,0:T(8,128)(2,1)} custom-call(bf16[640,1024]{1,0:T(8,128)(2,1)} %hidden_hbm.1, f32[1,2048]{1,0:T(1,128)} %bitcast.5, bf16[256,512]{1,0:T(8,128)(2,1)} %value_hbm.1, bf16[256,512]{1,0:T(8,128)(2,1)} %gate_hbm.1, f32[31,512]{1,0:T(8,128)} %taps.1, f32[1,512]{1,0:T(1,128)} %bitcast.7, f32[1,512]{1,0:T(1,128)} %bitcast.8, ...), custom_call_target="tpu_custom_call" | custom-call | tf_op jit(solution)/shard_map/pallas_call | solution.py:814
  179.9 2.5 %copy.14 = bf16[640,1024]{1,0:T(8,128)(2,1)} copy(bf16[640,1024]{1,0:T(8,128)(2,1)} %shard_map.118) | data formatting | bytes 2621440

commit v3 on v2

--- a/solution.py
+++ b/solution.py
@@ -431,9 +431,9 @@
         push(("yf", index), front_half(index, fy, rep), to_fy, when=when)
         push(("xf", 0, index), front_half(index, fy, rep), to_rep, when=when)
 
-    def front_turn(index):
-        recv(("yf", index), front_half(index, 1 - fy, rep))
-        push(("xf", 1, index), front_half(index, 1 - fy, rep), to_rep)
+    def front_turn(index, when=None):
+        recv(("yf", index), front_half(index, 1 - fy, rep), when=when)
+        push(("xf", 1, index), front_half(index, 1 - fy, rep), to_rep, when=when)
 
     def back_on(index):
         push(("yb", index), back_half(index, fy, back_side), to_fy)
@@ -466,8 +466,9 @@
     front_cross()
     push(("yf", 0, 1), front_half(0, fy, 1), to_fy, when=ends)
     line_relay("zb", lambda index: back_half(index, fy, back_side))
+    front_turn(3, middle)
     front_turn(2)
-    front_turn(3)
+    front_turn(3, ends)
     recv(("zb", 1), back_half(1, fy, back_side))
     back_on(1)
     recv(("zb", 2), back_half(2, fy, back_side))

time: 183 us -> 182 us (level)
  no operation moved by 1% of the time
where the time goes in v3:
time: 182 us
  Pallas kernels  180 us (99%)
  local copies, waits for them, and re-layouts  2.47 us (1%)
    pallas_call x1, Pallas kernels, fused(): pl.pallas_call(fused_kernel, out_shape=jax.ShapeDtypeStruct((tokens, half...  180 us

profile of v3, /device:TPU:0, one launch (start us, length us, event | category | flops | bytes accessed | tf_op | source)
XLA Modules:
  0.0 182.2 jit_solution(1145097221981608749)
XLA Ops:
  0.0 179.7 %shard_map.118 = bf16[640,1024]{1,0:T(8,128)(2,1)} custom-call(bf16[640,1024]{1,0:T(8,128)(2,1)} %hidden_hbm.1, f32[1,2048]{1,0:T(1,128)} %bitcast.5, bf16[256,512]{1,0:T(8,128)(2,1)} %value_hbm.1, bf16[256,512]{1,0:T(8,128)(2,1)} %gate_hbm.1, f32[31,512]{1,0:T(8,128)} %taps.1, f32[1,512]{1,0:T(1,128)} %bitcast.7, f32[1,512]{1,0:T(1,128)} %bitcast.8, ...), custom_call_target="tpu_custom_call" | custom-call | tf_op jit(solution)/shard_map/pallas_call | solution.py:815
  179.7 2.5 %copy.14 = bf16[640,1024]{1,0:T(8,128)(2,1)} copy(bf16[640,1024]{1,0:T(8,128)(2,1)} %shard_map.118) | data formatting | bytes 2621440
